TPU v7x, 32 devices: a whole 2x2x4 slice. The times are simulated.
32 devices in a mesh: sp: 8 (over z, y), tp: 4 (over x, core).
Axes of the slice: x: 2, y: 2, z: 4, core: 2. Of those that a mesh axis runs over, the one named last changes fastest.
Arguments:
- tokens: bfloat16 [1536, 2048], P(('sp', 'tp')), may hold values from -6 to 6
- norm_in: float32 [2048], replicated, may hold values from 0.1 to 1.9
- decay_log: float32 [128, 64], P('tp'), may hold values from -0.034 to -0.00016276042, as said below
- phase: float32 [128, 64], P('tp'), may hold values from -1 to 1
- b_real: float32 [128, 64, 16], P('tp'), may hold values from -1 to 1
- b_imag: float32 [128, 64, 16], P('tp'), may hold values from -1 to 1
- c_real: float32 [128, 16, 64], P('tp'), may hold values from -0.75 to 0.75
- c_imag: float32 [128, 16, 64], P('tp'), may hold values from -0.75 to 0.75
- skip_gain: float32 [2048], P('tp'), may hold values from -6 to 6
- w_value: bfloat16 [2048, 2048], P(None, 'tp'), as said below
- w_gate: bfloat16 [2048, 2048], P(None, 'tp'), may hold values from -0.125 to 0.125
- norm_out: float32 [2048], P('tp'), may hold values from 0.1 to 1.9
Outputs:
- mixed: bfloat16 [1536, 2048], P('sp', 'tp')
Inputs may be any that keep to these rules, and one draw needn't show every extreme that they name: `decay_log`: negative real parts of the eigenvalues. `w_value`: weights of the value projection.
All inputs are finite; a program needn't handle non-finite values.
Results may differ from a plain program's by a relative error of at most 0.012.
The roundings to bfloat16 on the way count: a program that leaves them out, or rounds other values in their place, can miss the bound.
Values may be sent and summed in bfloat16 or wider, within the bound.
A program may use at most 64 MiB of HBM per device.

v0:
```python
import jax
import jax.numpy as jnp
from jax import lax
from jax.sharding import PartitionSpec as P

D = 2048


NORM_EPS = 1e-06
HIGHEST_PREC = lax.Precision.HIGHEST


def entering(value, axis, join, neutral):
    count, mine = (lax.axis_size(axis), lax.axis_index(axis))
    pieces = jax.tree.map(lambda part: lax.all_gather(part, axis), value)
    subtotal = jax.tree.map(
        lambda part, zero: jnp.full_like(part, 0) + jnp.asarray(zero, part.dtype), value, neutral
    )

    def hop(position, subtotal):
        longer = join(subtotal, jax.tree.map(lambda part: part[position], pieces))
        return jax.tree.map(lambda new, old: jnp.where(position < mine, new, old), longer, subtotal)

    return lax.fori_loop(0, count - 1, hop, subtotal)


def coefficients(decay_log, phase, b_real, b_imag):
    magnitude = jnp.exp(decay_log)
    bar_re = magnitude * jnp.cos(phase)
    bar_im = magnitude * jnp.sin(phase)
    modulus = decay_log * decay_log + phase * phase
    coef_re = ((bar_re - 1.0) * decay_log + bar_im * phase) / modulus
    coef_im = (bar_im * decay_log - (bar_re - 1.0) * phase) / modulus
    in_re = coef_re[:, :, None] * b_real - coef_im[:, :, None] * b_imag
    in_im = coef_re[:, :, None] * b_imag + coef_im[:, :, None] * b_real
    return (bar_re, bar_im, in_re, in_im)


def prefix_states(drive_re, drive_im, rate_re, rate_im):
    length = drive_re.shape[0]
    stride = 1
    for level in range(max(length - 1, 1).bit_length()):
        padding = jnp.zeros((stride,) + drive_re.shape[1:], jnp.float32)
        moved_re = jnp.concatenate([padding, drive_re[: length - stride]], axis=0)
        moved_im = jnp.concatenate([padding, drive_im[: length - stride]], axis=0)
        drive_re, drive_im = (
            drive_re + rate_re * moved_re - rate_im * moved_im,
            drive_im + rate_re * moved_im + rate_im * moved_re,
        )
        rate_re, rate_im = (rate_re * rate_re - rate_im * rate_im, 2.0 * rate_re * rate_im)
        stride = stride * 2
    return (drive_re, drive_im)


def readout(state_re, state_im, c_real, c_imag):
    first = jnp.einsum("tgp,ghp->tgh", state_re, c_real, precision=HIGHEST_PREC)
    second = jnp.einsum("tgp,ghp->tgh", state_im, c_imag, precision=HIGHEST_PREC)
    return first - second


def powers(decay_log, phase, exponents):
    magnitude = jnp.exp(exponents[:, None, None] * decay_log[None])
    angles = exponents[:, None, None] * phase[None]
    return (magnitude * jnp.cos(angles), magnitude * jnp.sin(angles))


def combine(earlier, later):
    first_re, first_im, held_re, held_im = earlier
    second_re, second_im, own_re, own_im = later
    return (
        first_re * second_re - first_im * second_im,
        first_re * second_im + first_im * second_re,
        second_re * held_re - second_im * held_im + own_re,
        second_re * held_im + second_im * held_re + own_im,
    )


def on_device(
    tokens,
    norm_in,
    decay_log,
    phase,
    b_real,
    b_imag,
    c_real,
    c_imag,
    skip_gain,
    w_value,
    w_gate,
    norm_out,
):
    xf = tokens.astype(jnp.float32)
    normed = (xf * lax.rsqrt(jnp.mean(xf * xf, axis=1, keepdims=True) + NORM_EPS) * norm_in).astype(
        jnp.bfloat16
    )
    by_channel = lax.all_to_all(normed, "tp", split_axis=1, concat_axis=0, tiled=True)
    row_total, width = by_channel.shape
    groups = decay_log.shape[0]
    drive = by_channel.astype(jnp.float32).reshape(row_total, groups, width // groups)
    bar_re, bar_im, bb_re, bb_im = coefficients(decay_log, phase, b_real, b_imag)
    in_re = jnp.einsum("tgh,gph->tgp", drive, bb_re, precision=HIGHEST_PREC)
    in_im = jnp.einsum("tgh,gph->tgp", drive, bb_im, precision=HIGHEST_PREC)
    positions = jnp.arange(row_total, dtype=jnp.float32)
    back_re, back_im = powers(decay_log, phase, row_total - 1.0 - positions)
    end_re = jnp.sum(back_re * in_re - back_im * in_im, axis=0)
    end_im = jnp.sum(back_re * in_im + back_im * in_re, axis=0)
    whole_re, whole_im = powers(decay_log, phase, jnp.full((1,), row_total, jnp.float32))
    unity = jnp.ones_like(end_re)
    nothing = jnp.zeros_like(end_re)
    carried = entering(
        (whole_re[0], whole_im[0], end_re, end_im),
        "sp",
        combine,
        (unity, nothing, nothing, nothing),
    )
    held_re, held_im = (carried[2], carried[3])
    seeded_re = in_re.at[0].add(bar_re * held_re - bar_im * held_im)
    seeded_im = in_im.at[0].add(bar_re * held_im + bar_im * held_re)
    total_re, total_im = prefix_states(seeded_re, seeded_im, bar_re, bar_im)
    mixed_pre = readout(total_re, total_im, c_real, c_imag) + skip_gain.reshape(groups, -1) * drive
    z_local = jax.nn.gelu(mixed_pre).reshape(row_total, width).astype(jnp.bfloat16)
    shard_rows = lax.all_gather(z_local, "tp", axis=1, tiled=True)
    projected_value = jnp.dot(shard_rows, w_value, preferred_element_type=jnp.float32)
    projected_gate = jnp.dot(shard_rows, w_gate, preferred_element_type=jnp.float32)
    gated = projected_value * jax.nn.sigmoid(projected_gate)
    squares = lax.psum(jnp.sum(gated * gated, axis=1), "tp")
    scale = lax.rsqrt(squares / D + NORM_EPS)
    return (gated * scale[:, None] * norm_out).astype(jnp.bfloat16)


def solution(mesh):
    placed = (
        P(("sp", "tp"), None),
        P(),
        P("tp", None),
        P("tp", None),
        P("tp", None, None),
        P("tp", None, None),
        P("tp", None, None),
        P("tp", None, None),
        P("tp"),
        P(None, "tp"),
        P(None, "tp"),
        P("tp"),
    )
    return jax.shard_map(
        on_device, mesh=mesh, in_specs=placed, out_specs=P("sp", "tp"), check_vma=False
    )
```

profile of v0, /device:TPU:0, one launch (start us, length us, event | category | flops | bytes accessed | tf_op | source)
XLA Modules:
  0.0 203.8 jit_solution(2601990353164014799)
XLA Ops:
  0.0 0.0 copy-start
  0.0 1.2 fusion.47
  1.2 1.1 fusion.49
  2.3 0.7 copy.38
  3.0 4.2 %all-to-all-start = ((bf16[48,4,512]{2,0,1:T(8,128)(2,1)}), bf16[48,4,512]{2,0,1:T(8,128)(2,1)S(1)}, u32[]{:S(2)}, u32[]{:S(2)}) async-start(bf16[48,4,512]{2,0,1:T(8,128)(2,1)} %bitcast.63), calls=%async_computation | async-start | bytes 393216 | tf_op jit(solution)/shard_map/all_to_all | solution.py:96
  7.2 1.5 multiply_subtract_fusion.6
  8.7 1.4 fusion.62
  10.1 31.6 %all-gather = f32[256,64]{1,0:T(8,128)S(1)} all-gather(f32[32,64]{1,0:T(8,128)S(1)} %get-tuple-element.252), channel_id=2, replica_groups=mesh['sp'=8,'tp'=4] {'sp'}, dimensions={0}, use_global_device_ids=true | all-gather | bytes 73728 | tf_op jit(solution)/shard_map/all_gather | solution.py:15
  41.7 1.4 mul.652
  43.1 30.5 %all-gather.1 = f32[256,64]{1,0:T(8,128)S(1)} all-gather(f32[32,64]{1,0:T(8,128)S(1)} %get-tuple-element.251), channel_id=3, replica_groups=mesh['sp'=8,'tp'=4] {'sp'}, dimensions={0}, use_global_device_ids=true | all-gather | bytes 73728 | tf_op jit(solution)/shard_map/all_gather | solution.py:15
  73.6 0.5 iota_subtract_fusion
  74.1 0.0 all-to-all-done
  74.1 0.3 copy.33
  74.4 0.3 reshape.121
  74.7 0.0 copy-start.3
  74.8 0.0 copy-start.16
  74.8 0.0 copy-start.17
  74.8 0.0 copy-start.18
  74.8 0.0 copy-start.19
  74.8 0.0 copy-start.22
  74.8 0.0 copy-done.2
  74.8 2.1 %fusion.54 = f32[32,64,192]{2,1,0:T(8,128)S(1)} fusion(bf16[192,32,16]{0,2,1:T(8,128)(2,1)S(1)} %reshape.121, f32[32,64,16]{1,2,0:T(8,128)S(1)} %copy-done.2, f32[32,64,16]{1,2,0:T(8,128)} %param.22, f32[32,64]{1,0:T(8,128)} %get-tuple-element.250, f32[32,64]{1,0:T(8,128)} %get-tuple-element.249), kind=kOutput, calls=%fused_computation.81 | convolution fusion | flops 75595776 | bytes 2048000 | tf_op jit(solution)/shard_map/tgh,gph->tgp/dot_general | solution.py:101
  76.9 0.0 copy-done.3
  76.9 0.0 copy-done.16
  76.9 0.0 copy-done.17
  76.9 0.0 copy-done.18
  76.9 0.0 copy-done.19
  77.0 0.0 copy-done.22
  77.0 0.0 copy-start.1
  77.0 13.3 %add_reduce_fusion = (f32[32,64]{1,0:T(8,128)S(1)}, f32[32,64]{1,0:T(8,128)S(1)}, f32[32,64,192]{2,1,0:T(8,128)}) fusion(f32[32,64]{1,0:T(8,128)S(1)} %copy-done.18, f32[32,64]{1,0:T(8,128)S(1)} %copy-done.19, f32[192]{0:T(256)S(1)} %copy-done.22, f32[32,64,192]{2,1,0:T(8,128)S(1)} %fusion.54, bf16[192,32,16]{0,2,1:T(8,128)(2,1)S(1)} %reshape.121, ...), kind=kOutput, calls=%fused_computation.44 | convolution fusion | flops 80310272 | bytes 3654400 | tf_op jit(solution)/shard_map/tgh,gph->tgp/dot_general | solution.py:102
  90.3 0.0 copy-done.1
  90.3 30.5 %all-gather.2 = f32[256,64]{1,0:T(8,128)S(1)} all-gather(f32[32,64]{1,0:T(8,128)S(1)} %get-tuple-element.199), channel_id=4, replica_groups=mesh['sp'=8,'tp'=4] {'sp'}, dimensions={0}, use_global_device_ids=true | all-gather | bytes 73728 | tf_op jit(solution)/shard_map/all_gather | solution.py:15
  120.8 30.7 %all-gather.3 = f32[256,64]{1,0:T(8,128)S(1)} all-gather(f32[32,64]{1,0:T(8,128)S(1)} %get-tuple-element.198), channel_id=5, replica_groups=mesh['sp'=8,'tp'=4] {'sp'}, dimensions={0}, use_global_device_ids=true | all-gather | bytes 73728 | tf_op jit(solution)/shard_map/all_gather | solution.py:15
  151.5 0.3 while.18
  151.8 2.2 %slice_reduce_fusion = (f32[32,64]{1,0:T(8,128)S(1)}, f32[32,64]{1,0:T(8,128)S(1)}) fusion(f32[32,64,192]{2,1,0:T(8,128)} %get-tuple-element.253, f32[32,64,192]{2,1,0:T(8,128)} %copy-done.1), kind=kLoop, calls=%fused_computation.55 | loop fusion | bytes 32768 | tf_op jit(solution)/shard_map/slice.55
  154.0 1.4 copy.34
  155.4 0.4 copy.35
  155.8 3.7 %scatter-add.6 = f32[192,32,64]{0,2,1:T(8,128)} dynamic-update-slice(f32[192,32,64]{0,2,1:T(8,128)} %bitcast.82, f32[1,32,64]{0,2,1:T(8,128)} %copy.34, s32[]{:T(128)} %constant.103.clone.1, s32[]{:T(128)} %constant.103.clone.1, s32[]{:T(128)} %constant.103.clone.1) | dynamic-update-slice | bytes 16388 | tf_op jit(solution)/shard_map/scatter-add | solution.py:117
  159.5 3.5 %scatter-add.9 = f32[192,32,64]{0,2,1:T(8,128)} dynamic-update-slice(f32[192,32,64]{0,2,1:T(8,128)} %bitcast.94, f32[1,32,64]{0,2,1:T(8,128)S(1)} %copy.35, s32[]{:T(128)} %constant.103.clone.1, s32[]{:T(128)} %constant.103.clone.1, s32[]{:T(128)} %constant.103.clone.1) | dynamic-update-slice | bytes 16388 | tf_op jit(solution)/shard_map/scatter-add | solution.py:118
  163.0 5.3 %multiply_add_fusion.5 = (f32[192,32,64]{0,2,1:T(8,128)S(1)}, f32[192,32,64]{0,2,1:T(8,128)S(1)}) fusion(f32[192,32,64]{0,2,1:T(8,128)} %scatter-add.9, f32[191,32,64]{0,2,1:T(8,128)} %bitcast.95, f32[191,32,64]{0,2,1:T(8,128)} %bitcast.83, f32[32,64]{1,0:T(8,128)S(1)} %get-tuple-element.230, f32[32,64]{1,0:T(8,128)S(1)} %get-tuple-element.229, ...), kind=kLoop, calls=%fused_computation.42 | loop fusion | flops 3145728 | bytes 9437184 | tf_op jit(solution)/shard_map/add | solution.py:48
  168.3 0.0 copy-done.13
  168.4 0.0 copy-done.14
  168.4 0.0 copy-start.11
  168.4 1.9 multiply_add_fusion.4
  170.4 1.9 multiply_add_fusion.3
  172.3 1.9 multiply_add_fusion.2
  174.3 1.9 multiply_add_fusion.1
  176.2 1.9 multiply_add_fusion
  178.2 0.1 slice.124
  178.3 0.1 slice.125
  178.4 1.9 fusion.6
  180.3 0.0 copy-start.4
  180.3 0.1 slice.126
  180.4 0.1 slice.127
  180.5 0.8 copy-done.4
  181.2 1.8 fusion.10
  183.1 0.0 copy-start.21
  183.1 2.0 fusion.44
  185.1 10.5 %all_gather.27 = bf16[192,2048]{0,1:T(8,128)(2,1)S(1)} all-gather(bf16[192,512]{0,1:T(8,128)(2,1)S(1)} %bitcast.96), channel_id=1, replica_groups=mesh['sp'=8,'tp'=4] {'tp'}, dimensions={1}, use_global_device_ids=true | all-gather | bytes 983040 | tf_op jit(solution)/shard_map/all_gather | solution.py:122
  195.6 0.7 fusion.30
  196.3 0.0 copy-start.20
  196.3 0.7 multiply_reduce_fusion
  197.0 6.0 %psum.7 = f32[192]{0:T(256)S(1)} all-reduce(f32[192]{0:T(256)S(1)} %get-tuple-element.254), channel_id=1, replica_groups=mesh['sp'=8,'tp'=4] {'tp'}, use_global_device_ids=true, to_apply=%region_6.7 | all-reduce | flops 192 | bytes 1536 | tf_op jit(solution)/shard_map/psum | solution.py:126
  203.0 0.8 multiply_convert_fusion
  (36 shorter events, 0.2 us)
Async XLA Ops:
  0.0 196.3 %copy-start = (bf16[2048,512]{1,0:T(8,128)(2,1)S(1)}, bf16[2048,512]{1,0:T(8,128)(2,1)}, u32[]{:S(2)}) copy-start(bf16[2048,512]{1,0:T(8,128)(2,1)} %param.27) | copy-start | bytes 6291460
  0.0 74.8 %copy-start.2 = (f32[32,64,16]{1,2,0:T(8,128)S(1)}, f32[32,64,16]{1,2,0:T(8,128)}, u32[]{:S(2)}) copy-start(f32[32,64,16]{1,2,0:T(8,128)} %param.23) | copy-start | bytes 393220
  3.0 71.1 %all-to-all-start = ((bf16[48,4,512]{2,0,1:T(8,128)(2,1)}), bf16[48,4,512]{2,0,1:T(8,128)(2,1)S(1)}, u32[]{:S(2)}, u32[]{:S(2)}) async-start(bf16[48,4,512]{2,0,1:T(8,128)(2,1)} %bitcast.63), calls=%async_computation | async-start | bytes 393216 | tf_op jit(solution)/shard_map/all_to_all | solution.py:96
  74.7 2.2 %copy-start.3 = (f32[32,64,16]{1,2,0:T(8,128)S(1)}, f32[32,64,16]{1,2,0:T(8,128)}, u32[]{:S(2)}) copy-start(f32[32,64,16]{1,2,0:T(8,128)} %param.22) | copy-start | bytes 393220
  74.8 2.2 %copy-start.16 = (f32[32,64]{1,0:T(8,128)S(1)}, f32[32,64]{1,0:T(8,128)}, u32[]{:S(2)}) copy-start(f32[32,64]{1,0:T(8,128)} %get-tuple-element.249) | copy-start | bytes 24580
  74.8 2.2 %copy-start.17 = (f32[32,64]{1,0:T(8,128)S(1)}, f32[32,64]{1,0:T(8,128)}, u32[]{:S(2)}) copy-start(f32[32,64]{1,0:T(8,128)} %get-tuple-element.250) | copy-start | bytes 24580
  74.8 2.2 %copy-start.18 = (f32[32,64]{1,0:T(8,128)S(1)}, f32[32,64]{1,0:T(8,128)}, u32[]{:S(2)}) copy-start(f32[32,64]{1,0:T(8,128)} %param.21) | copy-start | bytes 24580
  74.8 2.2 %copy-start.19 = (f32[32,64]{1,0:T(8,128)S(1)}, f32[32,64]{1,0:T(8,128)}, u32[]{:S(2)}) copy-start(f32[32,64]{1,0:T(8,128)} %param.20) | copy-start | bytes 24580
  74.8 2.2 %copy-start.22 = (f32[192]{0:T(256)S(1)}, f32[192]{0:T(256)}, u32[]{:S(2)}) copy-start(f32[192]{0:T(256)} %iota_subtract_fusion) | copy-start | bytes 2308
  77.0 13.3 %copy-start.1 = (f32[32,64,192]{2,1,0:T(8,128)}, f32[32,64,192]{2,1,0:T(8,128)S(1)}, u32[]{:S(2)}) copy-start(f32[32,64,192]{2,1,0:T(8,128)S(1)} %fusion.54) | copy-start | bytes 4718596
  163.0 5.3 %copy-start.13 = (f32[32,64]{1,0:T(8,128)S(1)}, f32[32,64]{1,0:T(8,128)}, u32[]{:S(2)}) copy-start(f32[32,64]{1,0:T(8,128)} %get-tuple-element.227) | copy-start | bytes 24580
  163.0 5.3 %copy-start.14 = (f32[32,64]{1,0:T(8,128)S(1)}, f32[32,64]{1,0:T(8,128)}, u32[]{:S(2)}) copy-start(f32[32,64]{1,0:T(8,128)} %get-tuple-element.228) | copy-start | bytes 24580
  168.4 2.0 copy-start.11
  168.4 2.0 copy-start.12
  170.3 2.0 copy-start.9
  170.3 2.0 copy-start.10
  172.3 2.0 copy-start.7
  172.3 2.0 copy-start.8
  174.3 1.9 copy-start.6
  180.3 1.0 copy-start.4
  181.2 1.8 copy-start.5
  181.2 1.9 copy-start.15
  183.1 12.5 %copy-start.21 = (bf16[2048,512]{1,0:T(8,128)(2,1)S(1)}, bf16[2048,512]{1,0:T(8,128)(2,1)}, u32[]{:S(2)}) copy-start(bf16[2048,512]{1,0:T(8,128)(2,1)} %param.28) | copy-start | bytes 6291460
  196.3 6.7 %copy-start.20 = (f32[512]{0:T(512)S(1)}, f32[512]{0:T(512)}, u32[]{:S(2)}) copy-start(f32[512]{0:T(512)} %param.29) | copy-start | bytes 6148
where the time goes:
time: 204 us
  blocking collectives  140 us (69%)
  other arithmetic  23.5 us (12%)
  matrix products  20.6 us (10%)
  local copies, waits for them, and re-layouts  15.1 us (7%)
  starting transfers between devices  4.24 us (2%)
    all_gather x4, blocking collectives, entering(): pieces = jax.tree.map(lambda part: lax.all_gather(part, axis), value)  123 us
    add x7, other arithmetic, prefix_states(): drive_im + rate_re * moved_im + rate_im * moved_re  16.8 us
    dot_general x1, matrix products, on_device(): in_im = jnp.einsum('tgh,gph->tgp', drive, bb_im, precision=HIGHEST_PREC)  13.3 us
    all_gather x1, blocking collectives, on_device(): shard_rows = lax.all_gather(z_local, 'tp', axis=1, tiled=True)  10.5 us
    psum x1, blocking collectives, on_device(): squares = lax.psum(jnp.sum(gated * gated, axis=1), 'tp')  6.01 us
    all_to_all x1, starting transfers between devices, on_device(): lax.all_to_all(normed, 'tp', split_axis=1, concat_axis=0, tiled=True)  4.24 us
  transfers between devices with their start and end apart: 1, of which 0 were waited for; matrix products, arithmetic and copies ran while one was open for 2% of the time, Pallas kernels for 0%

commit v1 on v0

v1 whole, which is shorter than its diff:
```python
import functools

import jax
import jax.numpy as jnp
from jax import lax
from jax.experimental import pallas as pl
from jax.experimental.pallas import tpu as pltpu
from jax.sharding import PartitionSpec as P

NORM_EPS = 1e-06
LANES = 128
F32 = jnp.float32
BF16 = jnp.bfloat16
HIGHEST = lax.Precision.HIGHEST
NT = (((1,), (1,)), ((), ()))


def cmul(ar, ai, br, bi):
    return ar * br - ai * bi, ar * bi + ai * br


def remote(src, dst, send, recv, target):
    return pltpu.make_async_remote_copy(
        src_ref=src,
        dst_ref=dst,
        send_sem=send,
        recv_sem=recv,
        device_id=target,
        device_id_type=pl.DeviceIdType.MESH,
    )


def layer(
    n_sp, n_tp, state, group,
    tok, nin, dlog, phase, bre_h, bim_h, cre_h, cim_h, skip, wv_h, wg_h, nout,
    out,
    nsend, urecv, uf, ub, rows_a, rows_p, t1r, t1i, t2r, t2i, bs, cs, wbuf, ylocal,
    e_f, e_send, e_all, l_ref, zbuf, wv, wg, acc_v, acc_g, sq_all,
    bre, bim, cre, cim,
    load_sem, a_send, a_recv, e_ssem, e_rsem, z_send, z_recv, f_send, q_send, q_recv,
):
    sp, tp = lax.axis_index("sp"), lax.axis_index("tp")
    mine, d_model = tok.shape
    rows, width = uf.shape
    n_blk = width // LANES
    per = LANES // group
    lanes = per * state
    core = lax.rem(tp, 2)
    partner = tp + 1 - 2 * core
    n_chip = n_tp // 2

    barrier = pltpu.get_barrier_semaphore()
    for k in range(1, n_tp):
        pl.semaphore_signal(
            barrier, inc=1, device_id={"tp": lax.rem(tp + k, n_tp)},
            device_id_type=pl.DeviceIdType.MESH,
        )

    def greet(k, c):
        pl.semaphore_signal(
            barrier, inc=1, device_id={"sp": lax.rem(sp + k, n_sp)},
            device_id_type=pl.DeviceIdType.MESH,
        )
        return c

    lax.fori_loop(1, n_sp, greet, 0)

    loads = [
        pltpu.make_async_copy(src, dst, load_sem.at[i])
        for i, (src, dst) in enumerate(
            ((bre_h, bre), (bim_h, bim), (cre_h, cre), (cim_h, cim), (wv_h, wv), (wg_h, wg))
        )
    ]
    for copy in loads:
        copy.start()

    xf = tok[...].astype(F32)
    scale = lax.rsqrt(jnp.sum(xf * xf, axis=1, keepdims=True) / d_model + NORM_EPS)
    normed = (xf * scale * nin[...]).astype(BF16)
    for j in range(n_tp):
        nsend[j] = normed[:, j * width : (j + 1) * width]

    side = LANES // state
    for i in range(width // group // side):
        cut = slice(i * LANES, (i + 1) * LANES)
        for src, dst in ((dlog, rows_a), (phase, rows_p)):
            row = jnp.concatenate([src[i * side + k : i * side + k + 1, :] for k in range(side)], axis=1)
            dst[:, cut] = jnp.broadcast_to(row, (8, LANES))

    pl.semaphore_wait(barrier, n_tp - 1 + n_sp - 1)

    sends = []
    for k in range(1, n_tp):
        j = lax.rem(tp + n_tp - k, n_tp)
        copy = remote(nsend.at[j], urecv.at[tp], a_send.at[k], a_recv.at[tp], {"tp": j})
        copy.start()
        sends.append(copy)
    urecv[tp] = nsend[tp]

    for blk in range(n_blk):
        cut = slice(blk * lanes, (blk + 1) * lanes)
        a, p = rows_a[:, cut], rows_p[:, cut]
        k = lax.broadcasted_iota(jnp.int32, a.shape, 0).astype(F32)
        mag, cos, sin = jnp.exp(a), jnp.cos(p), jnp.sin(p)
        lr, li = mag * cos, mag * sin
        inv = jnp.exp(-a)
        nr, ni = inv * cos, -inv * sin
        mod = a * a + p * p
        cr = ((lr - 1.0) * a + li * p) / mod
        ci = (li * a - (lr - 1.0) * p) / mod
        one, zero = jnp.ones_like(a), jnp.zeros_like(a)
        pr, pi, mr, mi = one, zero, cr, ci
        sr, si, qr, qi = lr, li, nr, ni
        row = lax.broadcasted_iota(jnp.int32, a.shape, 0)
        for bit in range(3):
            on = lax.rem(row // (1 << bit), 2) == 1
            ar, ai = cmul(pr, pi, sr, si)
            pr, pi = jnp.where(on, ar, pr), jnp.where(on, ai, pi)
            ar, ai = cmul(mr, mi, qr, qi)
            mr, mi = jnp.where(on, ar, mr), jnp.where(on, ai, mi)
            sr, si = cmul(sr, si, sr, si)
            qr, qi = cmul(qr, qi, qr, qi)
        t2r[0:8, cut], t2i[0:8, cut], t1r[0:8, cut], t1i[0:8, cut] = pr, pi, mr, mi
        done = 8
        while done < rows:
            more = min(done, rows - done)
            for off in range(0, more, 8):
                src, dst = slice(off, off + 8), slice(done + off, done + off + 8)
                t2r[dst, cut], t2i[dst, cut] = cmul(t2r[src, cut], t2i[src, cut], sr, si)
                t1r[dst, cut], t1i[dst, cut] = cmul(t1r[src, cut], t1i[src, cut], qr, qi)
            sr, si = cmul(sr, si, sr, si)
            qr, qi = cmul(qr, qi, qr, qi)
            done += more
        lastr, lasti = t2r[rows - 1 : rows, cut], t2i[rows - 1 : rows, cut]
        wr, wi = cmul(lastr, lasti, lr[0:1], li[0:1])
        l_ref[blk : blk + 1, :] = wr
        l_ref[n_blk + blk : n_blk + blk + 1, :] = wi
        l_ref[2 * n_blk + blk : 2 * n_blk + blk + 1, :] = lr[0:1]
        l_ref[3 * n_blk + blk : 3 * n_blk + blk + 1, :] = li[0:1]

    for copy in loads[:4]:
        copy.wait()
    keep_c = (
        lax.broadcasted_iota(jnp.int32, (LANES, lanes), 0) // group
        == lax.broadcasted_iota(jnp.int32, (LANES, lanes), 1) // state
    )
    for blk in range(n_blk):
        for part, in_ref, out_ref in ((0, bre, cre), (1, bim, cim)):
            at = slice(part * lanes, (part + 1) * lanes)
            ch = slice(blk * LANES, (blk + 1) * LANES)
            b, c = in_ref[ch, :], out_ref[ch, :]
            wide = jnp.where(keep_c, jnp.concatenate([b] * per, axis=1), 0.0)
            bs[blk, :, at] = wide.astype(BF16)
            wide = jnp.where(keep_c, jnp.concatenate([c if part == 0 else -c] * per, axis=1), 0.0)
            cs[blk, :, at] = wide.astype(BF16)
    lower = (
        lax.broadcasted_iota(jnp.int32, (rows, rows), 0)
        >= lax.broadcasted_iota(jnp.int32, (rows, rows), 1)
    ).astype(BF16)

    for k in range(1, n_tp):
        j = lax.rem(tp + k, n_tp)
        remote(nsend.at[j], urecv.at[j], a_send.at[k], a_recv.at[j], {"tp": j}).wait_recv()
    for j in range(n_tp):
        uf[j * mine : (j + 1) * mine, :] = urecv[j].astype(F32)
    ub[...] = uf[...].astype(BF16)

    for blk in range(n_blk):
        cut = slice(blk * lanes, (blk + 1) * lanes)
        u = ub[:, blk * LANES : (blk + 1) * LANES]
        d = jnp.dot(u, bs[blk], preferred_element_type=F32)
        wr, wi = cmul(d[:, :lanes], d[:, lanes:], t1r[:, cut], t1i[:, cut])
        wbuf[blk, :, :lanes] = wr.astype(BF16)
        wbuf[blk, :, lanes:] = wi.astype(BF16)
        er, ei = cmul(
            jnp.sum(wr, axis=0, keepdims=True), jnp.sum(wi, axis=0, keepdims=True),
            t2r[rows - 1 : rows, cut], t2i[rows - 1 : rows, cut],
        )
        e_f[blk : blk + 1, :] = er
        e_f[n_blk + blk : n_blk + blk + 1, :] = ei
    e_send[...] = e_f[...].astype(BF16)

    def end_copy(j):
        return remote(e_send, e_all.at[sp], e_ssem.at[j], e_rsem.at[sp], {"sp": j})

    def send_end(k, c):
        end_copy(n_sp - 1 - k).start()
        return c

    lax.fori_loop(0, n_sp - 1 - sp, send_end, 0)

    for blk in range(n_blk):
        cut = slice(blk * lanes, (blk + 1) * lanes)
        s = jnp.dot(lower, wbuf[blk], preferred_element_type=F32)
        xr, xi = cmul(s[:, :lanes], s[:, lanes:], t2r[:, cut], t2i[:, cut])
        wbuf[blk, :, :lanes] = xr.astype(BF16)
        wbuf[blk, :, lanes:] = xi.astype(BF16)
        y = lax.dot_general(wbuf[blk], cs[blk], NT, preferred_element_type=F32)
        ch = slice(blk * LANES, (blk + 1) * LANES)
        ylocal[:, ch] = y + skip[:, ch] * uf[:, ch]

    def join(j, held):
        hr, hi = held
        remote(e_send, e_all.at[j], e_ssem.at[j], e_rsem.at[j], {"sp": j}).wait_recv()
        e = e_all[j].astype(F32)
        hr, hi = cmul(hr, hi, l_ref[:n_blk], l_ref[n_blk : 2 * n_blk])
        return hr + e[:n_blk], hi + e[n_blk:]

    nil = jnp.zeros((n_blk, lanes), F32)
    hr, hi = lax.fori_loop(0, sp, join, (nil, nil))
    hr, hi = cmul(hr, hi, l_ref[2 * n_blk : 3 * n_blk], l_ref[3 * n_blk :])

    for blk in range(n_blk):
        cut = slice(blk * lanes, (blk + 1) * lanes)
        ch = slice(blk * LANES, (blk + 1) * LANES)
        xr, xi = cmul(hr[blk : blk + 1], hi[blk : blk + 1], t2r[:, cut], t2i[:, cut])
        wbuf[blk, :, :lanes] = xr.astype(BF16)
        wbuf[blk, :, lanes:] = xi.astype(BF16)
        y = lax.dot_general(wbuf[blk], cs[blk], NT, preferred_element_type=F32)
        zbuf[tp, blk] = jax.nn.gelu(y + ylocal[:, ch]).astype(BF16)
        for k in range(1, n_chip):
            j = lax.rem(tp + 2 * k, n_tp)
            copy = remote(
                zbuf.at[tp, blk], zbuf.at[tp, blk], z_send.at[k, blk], z_recv.at[tp, blk], {"tp": j}
            )
            copy.start()
            sends.append(copy)
        copy = remote(
            zbuf.at[tp, blk], zbuf.at[tp, blk], z_send.at[0, blk], z_recv.at[tp, blk], {"tp": partner}
        )
        copy.start()
        sends.append(copy)

    for copy in loads[4:]:
        copy.wait()

    def arrived(j, blk):
        remote(
            zbuf.at[j, blk], zbuf.at[j, blk], z_send.at[0, blk], z_recv.at[j, blk], {"tp": partner}
        ).wait_recv()

    def project(j, blk, first=False):
        at = pl.ds(pl.multiple_of(j * width + blk * LANES, LANES), LANES)
        z = zbuf[j, blk]
        v = jnp.dot(z, wv[at, :], preferred_element_type=F32)
        g = jnp.dot(z, wg[at, :], preferred_element_type=F32)
        if first:
            acc_v[...], acc_g[...] = v, g
        else:
            acc_v[...] += v
            acc_g[...] += g

    for blk in range(n_blk):
        project(tp, blk, blk == 0)
    for blk in range(n_blk):
        arrived(partner, blk)
        project(partner, blk)
    late = []
    for blk in range(n_blk):
        for k in range(1, n_chip):
            j = lax.rem(tp + n_tp - 2 * k, n_tp)
            arrived(j, blk)
            copy = remote(
                zbuf.at[j, blk], zbuf.at[j, blk], f_send.at[k, blk], z_recv.at[j, blk], {"tp": partner}
            )
            copy.start()
            sends.append(copy)
            project(j, blk)
            late.append((lax.rem(partner + n_tp - 2 * k, n_tp), blk))
            if len(late) > 1:
                item = late.pop(0)
                arrived(*item)
                project(*item)
    for item in late:
        arrived(*item)
        project(*item)

    gated = acc_v[...] * jax.nn.sigmoid(acc_g[...])
    acc_v[...] = gated
    square = gated * gated
    part = square[:, :LANES]
    for blk in range(1, n_blk):
        part = part + square[:, blk * LANES : (blk + 1) * LANES]
    total = lax.dot_general(jnp.ones((8, LANES), F32), part, NT, precision=HIGHEST, preferred_element_type=F32)
    sq_all[tp] = total[0:1]
    for k in range(1, n_tp):
        j = lax.rem(tp + n_tp - k, n_tp)
        copy = remote(sq_all.at[tp], sq_all.at[tp], q_send.at[k], q_recv.at[tp], {"tp": j})
        copy.start()
        sends.append(copy)
    total = total[0:1]
    for k in range(1, n_tp):
        j = lax.rem(tp + k, n_tp)
        remote(sq_all.at[j], sq_all.at[j], q_send.at[k], q_recv.at[j], {"tp": j}).wait_recv()
        total = total + sq_all[j]
    scale = lax.rsqrt(total / d_model + NORM_EPS)
    eye = (
        lax.broadcasted_iota(jnp.int32, (rows, rows), 0)
        == lax.broadcasted_iota(jnp.int32, (rows, rows), 1)
    ).astype(F32)
    column = lax.dot_general(
        eye, jnp.broadcast_to(scale, (LANES, rows)), NT, precision=HIGHEST, preferred_element_type=F32
    )
    for blk in range(n_blk):
        ch = slice(blk * LANES, (blk + 1) * LANES)
        out[:, ch] = (acc_v[:, ch] * column * nout[:, ch]).astype(BF16)

    for copy in sends:
        copy.wait_send()

    def sent(j, c):
        end_copy(j).wait_send()
        return c

    lax.fori_loop(sp + 1, n_sp, sent, 0)


def solution(mesh):
    n_sp, n_tp = mesh.shape["sp"], mesh.shape["tp"]

    def on_device(
        tokens, norm_in, decay_log, phase, b_real, b_imag, c_real, c_imag, skip_gain, w_value, w_gate, norm_out
    ):
        mine, d_model = tokens.shape
        rows = mine * n_tp
        groups, state, group = b_real.shape
        width = groups * group
        n_blk = width // LANES
        lanes = LANES // group * state
        entries = groups * state
        vmem = pl.BlockSpec(memory_space=pltpu.VMEM)
        hbm = pl.BlockSpec(memory_space=pl.ANY)
        dma = pltpu.SemaphoreType.DMA
        return pl.pallas_call(
            functools.partial(layer, n_sp, n_tp, state, group),
            out_shape=jax.ShapeDtypeStruct((rows, width), BF16),
            in_specs=[vmem] * 4 + [hbm] * 4 + [vmem] + [hbm] * 2 + [vmem],
            out_specs=vmem,
            scratch_shapes=[
                pltpu.VMEM((n_tp, mine, width), BF16),
                pltpu.VMEM((n_tp, mine, width), BF16),
                pltpu.VMEM((rows, width), F32),
                pltpu.VMEM((rows, width), BF16),
                pltpu.VMEM((8, entries), F32),
                pltpu.VMEM((8, entries), F32),
                pltpu.VMEM((rows, entries), F32),
                pltpu.VMEM((rows, entries), F32),
                pltpu.VMEM((rows, entries), F32),
                pltpu.VMEM((rows, entries), F32),
                pltpu.VMEM((n_blk, LANES, 2 * lanes), BF16),
                pltpu.VMEM((n_blk, LANES, 2 * lanes), BF16),
                pltpu.VMEM((n_blk, rows, 2 * lanes), BF16),
                pltpu.VMEM((rows, width), F32),
                pltpu.VMEM((2 * n_blk, lanes), F32),
                pltpu.VMEM((2 * n_blk, lanes), BF16),
                pltpu.VMEM((n_sp, 2 * n_blk, lanes), BF16),
                pltpu.VMEM((4 * n_blk, lanes), F32),
                pltpu.VMEM((n_tp, n_blk, rows, LANES), BF16),
                pltpu.VMEM(w_value.shape, BF16),
                pltpu.VMEM(w_gate.shape, BF16),
                pltpu.VMEM((rows, width), F32),
                pltpu.VMEM((rows, width), F32),
                pltpu.VMEM((n_tp, 1, rows), F32),
                pltpu.VMEM((width, state), F32),
                pltpu.VMEM((width, state), F32),
                pltpu.VMEM((width, state), F32),
                pltpu.VMEM((width, state), F32),
                dma((6,)),
                dma((n_tp,)),
                dma((n_tp,)),
                dma((n_sp,)),
                dma((n_sp,)),
                dma((n_tp // 2, n_blk)),
                dma((n_tp, n_blk)),
                dma((n_tp // 2, n_blk)),
                dma((n_tp,)),
                dma((n_tp,)),
            ],
            compiler_params=pltpu.CompilerParams(collective_id=0, has_side_effects=True),
        )(
            tokens,
            norm_in.reshape(1, -1),
            decay_log,
            phase,
            b_real.transpose(0, 2, 1).reshape(width, state),
            b_imag.transpose(0, 2, 1).reshape(width, state),
            c_real.reshape(width, state),
            c_imag.reshape(width, state),
            skip_gain.reshape(1, -1),
            w_value,
            w_gate,
            norm_out.reshape(1, -1),
        )

    placed = (
        P(("sp", "tp"), None),
        P(),
        P("tp", None),
        P("tp", None),
        P("tp", None, None),
        P("tp", None, None),
        P("tp", None, None),
        P("tp", None, None),
        P("tp"),
        P(None, "tp"),
        P(None, "tp"),
        P("tp"),
    )
    return jax.shard_map(
        on_device, mesh=mesh, in_specs=placed, out_specs=P("sp", "tp"), check_vma=False
    )
```

time: 204 us -> 27.6 us (0.14)
  blocking collectives: 140 us -> 0 us
  Pallas kernels: 0 us -> 25.8 us
  other arithmetic: 23.5 us -> 0 us
  matrix products: 20.6 us -> 0 us
  local copies, waits for them, and re-layouts: 15.1 us -> 1.62 us
  starting transfers between devices: 4.24 us -> 0 us
    all_gather x5 -> x0, blocking collectives: 134 us -> none  [the longest x4 123 us: entering(): pieces = jax.tree.map(lambda part: lax.all_gather(part, axis), value)]
    pallas_call x0 -> x1, Pallas kernels: none -> 25.8 us  [on_device(): pl.pallas_call(functools.partial(layer, n_sp, n_tp, state, group), out_sh...]
    dot_general x6 -> x0, matrix products: 20.6 us -> none  [the longest x1 13.3 us: on_device(): in_im = jnp.einsum('tgh,gph->tgp', drive, bb_im, precision=HIGHEST_PREC)]
    add x8 -> x0, other arithmetic: 16.8 us -> none  [the longest x7 16.8 us: prefix_states(): drive_im + rate_re * moved_im + rate_im * moved_re]
    scatter-add x2 -> x0, local copies, waits for them, and re-layouts: 7.25 us -> none  [the longest x1 3.72 us: on_device(): seeded_re = in_re.at[0].add(bar_re * held_re - bar_im * held_im)]
    psum x1 -> x0, blocking collectives: 6.01 us -> none  [on_device(): squares = lax.psum(jnp.sum(gated * gated, axis=1), 'tp')]
    all_to_all x1 -> x0, starting transfers between devices: 4.24 us -> none  [on_device(): lax.all_to_all(normed, 'tp', split_axis=1, concat_axis=0, tiled=True)]
    another operation x1 -> x0, local copies, waits for them, and re-layouts: 2.16 us -> none
  transfers between devices with their start and end apart: 1 -> 0, of which waited for: 0 -> 0; matrix products, arithmetic and copies ran while one was open for 2% -> 0% of each run, Pallas kernels for 0% -> 0%
where the time goes in v1:
time: 27.6 us; the launch traced here: 27.4 us
  Pallas kernels  25.8 us (93%)
  local copies, waits for them, and re-layouts  1.62 us (6%)
    pallas_call x1, Pallas kernels, on_device(): pl.pallas_call(functools.partial(layer, n_sp, n_tp, state, group), out_sh...  25.8 us
    unnamed x1, local copies, waits for them, and re-layouts  1.62 us

profile of v1, /device:TPU:0, one launch (start us, length us, event | category | flops | bytes accessed | tf_op | source)
XLA Modules:
  0.0 27.4 jit_solution(10596404150005074426)
XLA Ops:
  0.0 25.8 %shard_map.118 = bf16[192,512]{1,0:T(8,128)(2,1)} custom-call(bf16[48,2048]{1,0:T(8,128)(2,1)} %tok.1, f32[1,2048]{1,0:T(1,128)} %bitcast.15, f32[32,64]{1,0:T(8,128)} %dlog.1, f32[32,64]{1,0:T(8,128)} %phase.1, f32[512,64]{1,0:T(8,128)} %bitcast.11, f32[512,64]{1,0:T(8,128)} %bitcast.12, f32[512,64]{1,0:T(8,128)} %bitcast.13, f32[512,64]{1,0:T(8,128)} %bitcast.14, ...), custom_call_target="tpu_custom_call" | custom-call | tf_op jit(solution)/shard_map/pallas_call | solution.py:334
  25.8 1.6 %copy.14 = bf16[192,512]{1,0:T(8,128)(2,1)} copy(bf16[192,512]{1,0:T(8,128)(2,1)} %shard_map.118) | data formatting | bytes 393216

commit v2 on v1

--- a/solution.py
+++ b/solution.py
@@ -32,11 +32,11 @@
 
 def layer(
     n_sp, n_tp, state, group,
-    tok, nin, dlog, phase, bre_h, bim_h, cre_h, cim_h, skip, wv_h, wg_h, nout,
+    tok_h, nin_h, dlog_h, phase_h, bre_h, bim_h, cre_h, cim_h, skip_h, wv_h, wg_h, nout_h,
     out,
-    nsend, urecv, uf, ub, rows_a, rows_p, t1r, t1i, t2r, t2i, bs, cs, wbuf, ylocal,
-    e_f, e_send, e_all, l_ref, zbuf, wv, wg, acc_v, acc_g, sq_all,
-    bre, bim, cre, cim,
+    nsend, urecv, uf, rows_a, rows_p, t1r, t1i, t2r, t2i, bs, cs, wbuf, ylocal,
+    e_send, e_all, l_ref, zbuf, wv, wg, acc_v, acc_g, sq_all,
+    bre, bim, cre, cim, tok, nin, dlog, phase, skip, nout,
     load_sem, a_send, a_recv, e_ssem, e_rsem, z_send, z_recv, f_send, q_send, q_recv,
 ):
     sp, tp = lax.axis_index("sp"), lax.axis_index("tp")
@@ -49,36 +49,45 @@
     partner = tp + 1 - 2 * core
     n_chip = n_tp // 2
 
+    loads = [
+        pltpu.make_async_copy(src, dst, load_sem.at[i])
+        for i, (src, dst) in enumerate(
+            (
+                (tok_h, tok), (nin_h, nin), (dlog_h, dlog), (phase_h, phase),
+                (bre_h, bre), (bim_h, bim), (cre_h, cre), (cim_h, cim),
+                (skip_h, skip), (nout_h, nout), (wv_h, wv), (wg_h, wg),
+            )
+        )
+    ]
+    for copy in loads[:4]:
+        copy.start()
+
     barrier = pltpu.get_barrier_semaphore()
+
+    def greet(k, c):
+        pl.semaphore_signal(
+            barrier, inc=1, device_id={"sp": k}, device_id_type=pl.DeviceIdType.MESH
+        )
+        return c
+
+    lax.fori_loop(0, sp, greet, 0)
     for k in range(1, n_tp):
         pl.semaphore_signal(
             barrier, inc=1, device_id={"tp": lax.rem(tp + k, n_tp)},
             device_id_type=pl.DeviceIdType.MESH,
         )
-
-    def greet(k, c):
-        pl.semaphore_signal(
-            barrier, inc=1, device_id={"sp": lax.rem(sp + k, n_sp)},
-            device_id_type=pl.DeviceIdType.MESH,
-        )
-        return c
-
-    lax.fori_loop(1, n_sp, greet, 0)
-
-    loads = [
-        pltpu.make_async_copy(src, dst, load_sem.at[i])
-        for i, (src, dst) in enumerate(
-            ((bre_h, bre), (bim_h, bim), (cre_h, cre), (cim_h, cim), (wv_h, wv), (wg_h, wg))
-        )
-    ]
-    for copy in loads:
+    for copy in loads[4:10]:
         copy.start()
+    for copy in loads[:4]:
+        copy.wait()
 
     xf = tok[...].astype(F32)
     scale = lax.rsqrt(jnp.sum(xf * xf, axis=1, keepdims=True) / d_model + NORM_EPS)
     normed = (xf * scale * nin[...]).astype(BF16)
     for j in range(n_tp):
-        nsend[j] = normed[:, j * width : (j + 1) * width]
+        for blk in range(n_blk):
+            at = j * width + blk * LANES
+            nsend[j, blk] = normed[:, at : at + LANES]
 
     side = LANES // state
     for i in range(width // group // side):
@@ -86,16 +95,6 @@
         for src, dst in ((dlog, rows_a), (phase, rows_p)):
             row = jnp.concatenate([src[i * side + k : i * side + k + 1, :] for k in range(side)], axis=1)
             dst[:, cut] = jnp.broadcast_to(row, (8, LANES))
-
-    pl.semaphore_wait(barrier, n_tp - 1 + n_sp - 1)
-
-    sends = []
-    for k in range(1, n_tp):
-        j = lax.rem(tp + n_tp - k, n_tp)
-        copy = remote(nsend.at[j], urecv.at[tp], a_send.at[k], a_recv.at[tp], {"tp": j})
-        copy.start()
-        sends.append(copy)
-    urecv[tp] = nsend[tp]
 
     for blk in range(n_blk):
         cut = slice(blk * lanes, (blk + 1) * lanes)
@@ -138,7 +137,22 @@
         l_ref[2 * n_blk + blk : 2 * n_blk + blk + 1, :] = lr[0:1]
         l_ref[3 * n_blk + blk : 3 * n_blk + blk + 1, :] = li[0:1]
 
-    for copy in loads[:4]:
+    pl.semaphore_wait(barrier, n_tp - 1 + n_sp - 1 - sp)
+
+    sends = []
+    for blk in range(n_blk):
+        for k in range(1, n_tp):
+            j = lax.rem(tp + n_tp - k, n_tp)
+            copy = remote(
+                nsend.at[j, blk], urecv.at[tp, blk], a_send.at[k, blk], a_recv.at[tp, blk], {"tp": j}
+            )
+            copy.start()
+            sends.append(copy)
+    for copy in loads[10:]:
+        copy.start()
+    urecv[tp] = nsend[tp]
+
+    for copy in loads[4:10]:
         copy.wait()
     keep_c = (
         lax.broadcasted_iota(jnp.int32, (LANES, lanes), 0) // group
@@ -158,16 +172,22 @@
         >= lax.broadcasted_iota(jnp.int32, (rows, rows), 1)
     ).astype(BF16)
 
-    for k in range(1, n_tp):
-        j = lax.rem(tp + k, n_tp)
-        remote(nsend.at[j], urecv.at[j], a_send.at[k], a_recv.at[j], {"tp": j}).wait_recv()
-    for j in range(n_tp):
-        uf[j * mine : (j + 1) * mine, :] = urecv[j].astype(F32)
-    ub[...] = uf[...].astype(BF16)
+    def end_copy(j, blk):
+        return remote(
+            e_send.at[blk], e_all.at[sp, blk], e_ssem.at[j, blk], e_rsem.at[sp, blk], {"sp": j}
+        )
 
     for blk in range(n_blk):
         cut = slice(blk * lanes, (blk + 1) * lanes)
-        u = ub[:, blk * LANES : (blk + 1) * LANES]
+        ch = slice(blk * LANES, (blk + 1) * LANES)
+        for k in range(1, n_tp):
+            j = lax.rem(tp + k, n_tp)
+            remote(
+                nsend.at[j, blk], urecv.at[j, blk], a_send.at[k, blk], a_recv.at[j, blk], {"tp": j}
+            ).wait_recv()
+        for j in range(n_tp):
+            uf[j * mine : (j + 1) * mine, ch] = urecv[j, blk].astype(F32)
+        u = uf[:, ch].astype(BF16)
         d = jnp.dot(u, bs[blk], preferred_element_type=F32)
         wr, wi = cmul(d[:, :lanes], d[:, lanes:], t1r[:, cut], t1i[:, cut])
         wbuf[blk, :, :lanes] = wr.astype(BF16)
@@ -176,18 +196,13 @@
             jnp.sum(wr, axis=0, keepdims=True), jnp.sum(wi, axis=0, keepdims=True),
             t2r[rows - 1 : rows, cut], t2i[rows - 1 : rows, cut],
         )
-        e_f[blk : blk + 1, :] = er
-        e_f[n_blk + blk : n_blk + blk + 1, :] = ei
-    e_send[...] = e_f[...].astype(BF16)
-
-    def end_copy(j):
-        return remote(e_send, e_all.at[sp], e_ssem.at[j], e_rsem.at[sp], {"sp": j})
-
-    def send_end(k, c):
-        end_copy(n_sp - 1 - k).start()
-        return c
-
-    lax.fori_loop(0, n_sp - 1 - sp, send_end, 0)
+        e_send[blk] = jnp.concatenate([er, ei], axis=0).astype(BF16)
+
+        def send_end(k, c, blk=blk):
+            end_copy(n_sp - 1 - k, blk).start()
+            return c
+
+        lax.fori_loop(0, n_sp - 1 - sp, send_end, 0)
 
     for blk in range(n_blk):
         cut = slice(blk * lanes, (blk + 1) * lanes)
@@ -199,21 +214,25 @@
         ch = slice(blk * LANES, (blk + 1) * LANES)
         ylocal[:, ch] = y + skip[:, ch] * uf[:, ch]
 
-    def join(j, held):
-        hr, hi = held
-        remote(e_send, e_all.at[j], e_ssem.at[j], e_rsem.at[j], {"sp": j}).wait_recv()
-        e = e_all[j].astype(F32)
-        hr, hi = cmul(hr, hi, l_ref[:n_blk], l_ref[n_blk : 2 * n_blk])
-        return hr + e[:n_blk], hi + e[n_blk:]
-
-    nil = jnp.zeros((n_blk, lanes), F32)
-    hr, hi = lax.fori_loop(0, sp, join, (nil, nil))
-    hr, hi = cmul(hr, hi, l_ref[2 * n_blk : 3 * n_blk], l_ref[3 * n_blk :])
-
     for blk in range(n_blk):
         cut = slice(blk * lanes, (blk + 1) * lanes)
         ch = slice(blk * LANES, (blk + 1) * LANES)
-        xr, xi = cmul(hr[blk : blk + 1], hi[blk : blk + 1], t2r[:, cut], t2i[:, cut])
+        lr, li = l_ref[blk : blk + 1, :], l_ref[n_blk + blk : n_blk + blk + 1, :]
+
+        def join(j, held, blk=blk, lr=lr, li=li):
+            remote(
+                e_send.at[blk], e_all.at[j, blk], e_ssem.at[j, blk], e_rsem.at[j, blk], {"sp": j}
+            ).wait_recv()
+            e = e_all[j, blk].astype(F32)
+            hr, hi = cmul(*held, lr, li)
+            return hr + e[0:1], hi + e[1:2]
+
+        nil = jnp.zeros((1, lanes), F32)
+        hr, hi = lax.fori_loop(0, sp, join, (nil, nil))
+        hr, hi = cmul(
+            hr, hi, l_ref[2 * n_blk + blk : 2 * n_blk + blk + 1, :], l_ref[3 * n_blk + blk : 3 * n_blk + blk + 1, :]
+        )
+        xr, xi = cmul(hr, hi, t2r[:, cut], t2i[:, cut])
         wbuf[blk, :, :lanes] = xr.astype(BF16)
         wbuf[blk, :, lanes:] = xi.astype(BF16)
         y = lax.dot_general(wbuf[blk], cs[blk], NT, preferred_element_type=F32)
@@ -231,7 +250,7 @@
         copy.start()
         sends.append(copy)
 
-    for copy in loads[4:]:
+    for copy in loads[10:]:
         copy.wait()
 
     def arrived(j, blk):
@@ -309,7 +328,8 @@
         copy.wait_send()
 
     def sent(j, c):
-        end_copy(j).wait_send()
+        for blk in range(n_blk):
+            end_copy(j, blk).wait_send()
         return c
 
     lax.fori_loop(sp + 1, n_sp, sent, 0)
@@ -334,13 +354,12 @@
         return pl.pallas_call(
             functools.partial(layer, n_sp, n_tp, state, group),
             out_shape=jax.ShapeDtypeStruct((rows, width), BF16),
-            in_specs=[vmem] * 4 + [hbm] * 4 + [vmem] + [hbm] * 2 + [vmem],
+            in_specs=[hbm] * 12,
             out_specs=vmem,
             scratch_shapes=[
-                pltpu.VMEM((n_tp, mine, width), BF16),
-                pltpu.VMEM((n_tp, mine, width), BF16),
+                pltpu.VMEM((n_tp, n_blk, mine, LANES), BF16),
+                pltpu.VMEM((n_tp, n_blk, mine, LANES), BF16),
                 pltpu.VMEM((rows, width), F32),
-                pltpu.VMEM((rows, width), BF16),
                 pltpu.VMEM((8, entries), F32),
                 pltpu.VMEM((8, entries), F32),
                 pltpu.VMEM((rows, entries), F32),
@@ -351,9 +370,8 @@
                 pltpu.VMEM((n_blk, LANES, 2 * lanes), BF16),
                 pltpu.VMEM((n_blk, rows, 2 * lanes), BF16),
                 pltpu.VMEM((rows, width), F32),
-                pltpu.VMEM((2 * n_blk, lanes), F32),
-                pltpu.VMEM((2 * n_blk, lanes), BF16),
-                pltpu.VMEM((n_sp, 2 * n_blk, lanes), BF16),
+                pltpu.VMEM((n_blk, 2, lanes), BF16),
+                pltpu.VMEM((n_sp, n_blk, 2, lanes), BF16),
                 pltpu.VMEM((4 * n_blk, lanes), F32),
                 pltpu.VMEM((n_tp, n_blk, rows, LANES), BF16),
                 pltpu.VMEM(w_value.shape, BF16),
@@ -365,11 +383,17 @@
                 pltpu.VMEM((width, state), F32),
                 pltpu.VMEM((width, state), F32),
                 pltpu.VMEM((width, state), F32),
-                dma((6,)),
-                dma((n_tp,)),
-                dma((n_tp,)),
-                dma((n_sp,)),
-                dma((n_sp,)),
+                pltpu.VMEM((mine, d_model), BF16),
+                pltpu.VMEM((1, d_model), F32),
+                pltpu.VMEM((groups, state), F32),
+                pltpu.VMEM((groups, state), F32),
+                pltpu.VMEM((1, width), F32),
+                pltpu.VMEM((1, width), F32),
+                dma((12,)),
+                dma((n_tp, n_blk)),
+                dma((n_tp, n_blk)),
+                dma((n_sp, n_blk)),
+                dma((n_sp, n_blk)),
                 dma((n_tp // 2, n_blk)),
                 dma((n_tp, n_blk)),
                 dma((n_tp // 2, n_blk)),

time: 27.6 us -> 27.6 us (level)
  no operation moved by 1% of the time
where the time goes in v2:
time: 27.6 us; the launch traced here: 27.4 us
  Pallas kernels  25.8 us (93%)
  local copies, waits for them, and re-layouts  1.62 us (6%)
    pallas_call x1, Pallas kernels, on_device(): pl.pallas_call(functools.partial(layer, n_sp, n_tp, state, group), out_sh...  25.8 us
    unnamed x1, local copies, waits for them, and re-layouts  1.62 us

profile of v2, /device:TPU:0, one launch (start us, length us, event | category | flops | bytes accessed | tf_op | source)
XLA Modules:
  0.0 27.4 jit_solution(16805632688310985232)
XLA Ops:
  0.0 25.8 %shard_map.118 = bf16[192,512]{1,0:T(8,128)(2,1)} custom-call(bf16[48,2048]{1,0:T(8,128)(2,1)} %tok_h.1, f32[1,2048]{1,0:T(1,128)} %bitcast.15, f32[32,64]{1,0:T(8,128)} %dlog_h.1, f32[32,64]{1,0:T(8,128)} %phase_h.1, f32[512,64]{1,0:T(8,128)} %bitcast.11, f32[512,64]{1,0:T(8,128)} %bitcast.12, f32[512,64]{1,0:T(8,128)} %bitcast.13, f32[512,64]{1,0:T(8,128)} %bitcast.14, ...), custom_call_target="tpu_custom_call" | custom-call | tf_op jit(solution)/shard_map/pallas_call | solution.py:354
  25.8 1.6 %copy.14 = bf16[192,512]{1,0:T(8,128)(2,1)} copy(bf16[192,512]{1,0:T(8,128)(2,1)} %shard_map.118) | data formatting | bytes 393216

commit v3 on v2

--- a/solution.py
+++ b/solution.py
@@ -37,7 +37,7 @@
     nsend, urecv, uf, rows_a, rows_p, t1r, t1i, t2r, t2i, bs, cs, wbuf, ylocal,
     e_send, e_all, l_ref, zbuf, wv, wg, acc_v, acc_g, sq_all,
     bre, bim, cre, cim, tok, nin, dlog, phase, skip, nout,
-    load_sem, a_send, a_recv, e_ssem, e_rsem, z_send, z_recv, f_send, q_send, q_recv,
+    load_sem, a_send, a_recv, e_ssem, e_rsem, z_send, z_recv, f_send, q_send, q_recv, met,
 ):
     sp, tp = lax.axis_index("sp"), lax.axis_index("tp")
     mine, d_model = tok.shape
@@ -64,13 +64,19 @@
 
     barrier = pltpu.get_barrier_semaphore()
 
-    def greet(k, c):
-        pl.semaphore_signal(
-            barrier, inc=1, device_id={"sp": k}, device_id_type=pl.DeviceIdType.MESH
-        )
-        return c
-
-    lax.fori_loop(0, sp, greet, 0)
+    def signal_sp(sem, d):
+        for ok, to in ((sp >= d, sp - d), (sp + d < n_sp, sp + d)):
+
+            @pl.when(ok)
+            def _(to=to):
+                pl.semaphore_signal(
+                    sem, inc=1, device_id={"sp": to}, device_id_type=pl.DeviceIdType.MESH
+                )
+
+    def around(d):
+        return jnp.where(sp >= d, 1, 0) + jnp.where(sp + d < n_sp, 1, 0)
+
+    signal_sp(barrier, 1)
     for k in range(1, n_tp):
         pl.semaphore_signal(
             barrier, inc=1, device_id={"tp": lax.rem(tp + k, n_tp)},
@@ -137,7 +143,7 @@
         l_ref[2 * n_blk + blk : 2 * n_blk + blk + 1, :] = lr[0:1]
         l_ref[3 * n_blk + blk : 3 * n_blk + blk + 1, :] = li[0:1]
 
-    pl.semaphore_wait(barrier, n_tp - 1 + n_sp - 1 - sp)
+    pl.semaphore_wait(barrier, n_tp - 1 + around(1))
 
     sends = []
     for blk in range(n_blk):
@@ -148,6 +154,8 @@
             )
             copy.start()
             sends.append(copy)
+    if n_sp > 2:
+        signal_sp(met.at[0], 1)
     for copy in loads[10:]:
         copy.start()
     urecv[tp] = nsend[tp]
@@ -171,6 +179,16 @@
         lax.broadcasted_iota(jnp.int32, (rows, rows), 0)
         >= lax.broadcasted_iota(jnp.int32, (rows, rows), 1)
     ).astype(BF16)
+
+    d = 1
+    hops = []
+    while d < n_sp - 1:
+        hops.append(d)
+        d *= 2
+    for r, d in enumerate(hops):
+        if r > 0:
+            signal_sp(met.at[r], d)
+        pl.semaphore_wait(met.at[r], around(d))
 
     def end_copy(j, blk):
         return remote(
@@ -353,7 +371,7 @@
         dma = pltpu.SemaphoreType.DMA
         return pl.pallas_call(
             functools.partial(layer, n_sp, n_tp, state, group),
-            out_shape=jax.ShapeDtypeStruct((rows, width), BF16),
+            out_shape=pltpu.VMEM((rows, width), BF16),
             in_specs=[hbm] * 12,
             out_specs=vmem,
             scratch_shapes=[
@@ -399,6 +417,7 @@
                 dma((n_tp // 2, n_blk)),
                 dma((n_tp,)),
                 dma((n_tp,)),
+                pltpu.SemaphoreType.REGULAR((max(n_sp.bit_length(), 1),)),
             ],
             compiler_params=pltpu.CompilerParams(collective_id=0, has_side_effects=True),
         )(

time: 27.6 us -> 25.5 us (0.924)
  Pallas kernels: 25.8 us -> 24.7 us
  local copies, waits for them, and re-layouts: 1.62 us -> 0.68 us
    pallas_call x1, Pallas kernels: 25.8 us -> 24.7 us  [on_device(): pl.pallas_call(functools.partial(layer, n_sp, n_tp, state, group), out_sh...]
    unnamed x1, local copies, waits for them, and re-layouts: 1.62 us -> 0.68 us
where the time goes in v3:
time: 25.5 us; the launch traced here: 25.4 us
  Pallas kernels  24.7 us (97%)
  local copies, waits for them, and re-layouts  0.68 us (3%)
    pallas_call x1, Pallas kernels, on_device(): pl.pallas_call(functools.partial(layer, n_sp, n_tp, state, group), out_sh...  24.7 us
    unnamed x1, local copies, waits for them, and re-layouts  0.68 us

profile of v3, /device:TPU:0, one launch (start us, length us, event | category | flops | bytes accessed | tf_op | source)
XLA Modules:
  0.0 25.4 jit_solution(17008992412020241962)
XLA Ops:
  0.0 24.7 %shard_map.118 = bf16[192,512]{1,0:T(8,128)(2,1)S(1)} custom-call(bf16[48,2048]{1,0:T(8,128)(2,1)} %tok_h.1, f32[1,2048]{1,0:T(1,128)} %bitcast.15, f32[32,64]{1,0:T(8,128)} %dlog_h.1, f32[32,64]{1,0:T(8,128)} %phase_h.1, f32[512,64]{1,0:T(8,128)} %bitcast.11, f32[512,64]{1,0:T(8,128)} %bitcast.12, f32[512,64]{1,0:T(8,128)} %bitcast.13, f32[512,64]{1,0:T(8,128)} %bitcast.14, ...), custom_call_target="tpu_custom_call" | custom-call | tf_op jit(solution)/shard_map/pallas_call | solution.py:372
  24.7 0.7 %copy.14 = bf16[192,512]{1,0:T(8,128)(2,1)} copy(bf16[192,512]{1,0:T(8,128)(2,1)S(1)} %shard_map.118) | data formatting | bytes 393216

commit v4 on v3

--- a/solution.py
+++ b/solution.py
@@ -11,12 +11,21 @@
 LANES = 128
 F32 = jnp.float32
 BF16 = jnp.bfloat16
-HIGHEST = lax.Precision.HIGHEST
 NT = (((1,), (1,)), ((), ()))
 
 
 def cmul(ar, ai, br, bi):
     return ar * br - ai * bi, ar * bi + ai * br
+
+
+def exact(ones, value):
+    total = None
+    for _ in range(3):
+        term = value.astype(BF16)
+        value = value - term.astype(F32)
+        dot = lax.dot_general(ones, term, NT, preferred_element_type=F32)
+        total = dot if total is None else total + dot
+    return total
 
 
 def remote(src, dst, send, recv, target):
@@ -188,7 +197,8 @@
     for r, d in enumerate(hops):
         if r > 0:
             signal_sp(met.at[r], d)
-        pl.semaphore_wait(met.at[r], around(d))
+        if r < len(hops) - 1:
+            pl.semaphore_wait(met.at[r], around(d))
 
     def end_copy(j, blk):
         return remote(
@@ -216,6 +226,9 @@
         )
         e_send[blk] = jnp.concatenate([er, ei], axis=0).astype(BF16)
 
+        if blk == 0 and hops:
+            pl.semaphore_wait(met.at[len(hops) - 1], around(hops[-1]))
+
         def send_end(k, c, blk=blk):
             end_copy(n_sp - 1 - k, blk).start()
             return c
@@ -318,7 +331,7 @@
     part = square[:, :LANES]
     for blk in range(1, n_blk):
         part = part + square[:, blk * LANES : (blk + 1) * LANES]
-    total = lax.dot_general(jnp.ones((8, LANES), F32), part, NT, precision=HIGHEST, preferred_element_type=F32)
+    total = exact(jnp.ones((8, LANES), BF16), part)
     sq_all[tp] = total[0:1]
     for k in range(1, n_tp):
         j = lax.rem(tp + n_tp - k, n_tp)
@@ -334,10 +347,8 @@
     eye = (
         lax.broadcasted_iota(jnp.int32, (rows, rows), 0)
         == lax.broadcasted_iota(jnp.int32, (rows, rows), 1)
-    ).astype(F32)
-    column = lax.dot_general(
-        eye, jnp.broadcast_to(scale, (LANES, rows)), NT, precision=HIGHEST, preferred_element_type=F32
-    )
+    ).astype(BF16)
+    column = exact(eye, jnp.broadcast_to(scale, (LANES, rows)))
     for blk in range(n_blk):
         ch = slice(blk * LANES, (blk + 1) * LANES)
         out[:, ch] = (acc_v[:, ch] * column * nout[:, ch]).astype(BF16)

time: 25.5 us -> 24.8 us (0.973)
  Pallas kernels: 24.7 us -> 24 us
    pallas_call x1, Pallas kernels: 24.7 us -> 24 us  [on_device(): pl.pallas_call(functools.partial(layer, n_sp, n_tp, state, group), out_sh...]
where the time goes in v4:
time: 24.8 us; the launch traced here: 24.7 us
  Pallas kernels  24 us (97%)
  local copies, waits for them, and re-layouts  0.68 us (3%)
    pallas_call x1, Pallas kernels, on_device(): pl.pallas_call(functools.partial(layer, n_sp, n_tp, state, group), out_sh...  24 us
    unnamed x1, local copies, waits for them, and re-layouts  0.68 us

profile of v4, /device:TPU:0, one launch (start us, length us, event | category | flops | bytes accessed | tf_op | source)
XLA Modules:
  0.0 24.7 jit_solution(11874857493412559247)
XLA Ops:
  0.0 24.0 %shard_map.118 = bf16[192,512]{1,0:T(8,128)(2,1)S(1)} custom-call(bf16[48,2048]{1,0:T(8,128)(2,1)} %tok_h.1, f32[1,2048]{1,0:T(1,128)} %bitcast.15, f32[32,64]{1,0:T(8,128)} %dlog_h.1, f32[32,64]{1,0:T(8,128)} %phase_h.1, f32[512,64]{1,0:T(8,128)} %bitcast.11, f32[512,64]{1,0:T(8,128)} %bitcast.12, f32[512,64]{1,0:T(8,128)} %bitcast.13, f32[512,64]{1,0:T(8,128)} %bitcast.14, ...), custom_call_target="tpu_custom_call" | custom-call | tf_op jit(solution)/shard_map/pallas_call | solution.py:383
  24.0 0.7 %copy.14 = bf16[192,512]{1,0:T(8,128)(2,1)} copy(bf16[192,512]{1,0:T(8,128)(2,1)S(1)} %shard_map.118) | data formatting | bytes 393216
